TPU v7x, 32 devices: a whole 2x2x4 slice. The times are simulated.
32 devices in a mesh: grp: 2 (over y), sp: 4 (over z), tp: 4 (over x, core).
Axes of the slice: x: 2, y: 2, z: 4, core: 2. Of those that a mesh axis runs over, the one named last changes fastest.
Arguments:
- queries: bfloat16 [2048, 2048], P(('grp', 'sp'), 'tp'), parts along dimension 0, may hold values from -6 to 6
- keys: bfloat16 [2048, 512], P(('grp', 'sp'), 'tp'), parts along dimension 0, may hold values from -6 to 6
- values: bfloat16 [2048, 512], P(('grp', 'sp'), 'tp'), parts along dimension 0, may hold values from -6 to 6
- query_gain: float32 [128], replicated, may hold values from 1 to 5, as said below
- key_norm_gain: float32 [128], replicated, may hold values from 1 to 5, as said below
- out_weight: bfloat16 [2048, 2048], P('tp'), may hold values from -0.125 to 0.125
- residual: bfloat16 [2048, 2048], P(('grp', 'sp')), parts along dimension 0, may hold values from -0.59765625 to 0.59765625
- mixer_gain: float32 [2048], replicated, may hold values from 0.1 to 1.9
- gate_weight: bfloat16 [2048, 5632], P('sp', 'tp'), may hold values from -0.125 to 0.125
- up_weight: bfloat16 [2048, 5632], P('sp', 'tp'), may hold values from -0.125 to 0.125
- conv_taps: float32 [3, 5632], P(None, 'tp'), may hold values from -3.5 to 3.5
- down_weight: bfloat16 [5632, 2048], P('tp', 'sp'), may hold values from -0.078125 to 0.078125
Outputs:
- layer_out: bfloat16 [2048, 2048], P(('grp', 'sp', 'tp')), parts along dimension 0
There are 2 independent parts, one for each index of `grp`. A program takes and returns all parts, laid end to end along the dimension named above; an argument that names none is the same for every part. Nothing has to cross between parts.
Inputs may be any that keep to these rules, and one draw needn't show every extreme that they name: `query_gain`: positive. `key_norm_gain`: positive.
All inputs are finite; a program needn't handle non-finite values.
Results may differ from a plain program's by a relative error of at most 0.024.
Values may be sent and summed in bfloat16 or wider, within the bound.
A program may use at most 128 MiB of HBM per device.

v0:
```python
import math
import jax
import jax.numpy as jnp
from jax import lax
from jax.sharding import PartitionSpec as P

GRID = 64
norm_eps = 1e-06
rope_base = 10000.0


def padded_2(block, sides, width):
    for axis, dim in sides:
        count = lax.axis_size(axis)
        forward = [(i, i + 1) for i in range(count - 1)]
        backward = [(target, source) for source, target in forward]
        low = lax.ppermute(
            lax.slice_in_dim(block, block.shape[dim] - width, None, axis=dim), axis, forward
        )
        high = lax.ppermute(lax.slice_in_dim(block, 0, width, axis=dim), axis, backward)
        block = jnp.concatenate([low, block, high], axis=dim)
    return block


def angle_tables(positions, head_dim):
    quarter = head_dim // 4
    freqs = 1.0 / rope_base ** (jnp.arange(quarter, dtype=jnp.float32) * 4.0 / head_dim)
    grid_row = (positions // GRID).astype(jnp.float32)
    grid_col = (positions % GRID).astype(jnp.float32)
    by_row = grid_row[:, None] * freqs[None, :]
    by_col = grid_col[:, None] * freqs[None, :]
    angles = jnp.concatenate([by_row, by_row, by_col, by_col], axis=-1)
    return (jnp.cos(angles), jnp.sin(angles))


def apply_rotary(field, cosine_table, sine_table):
    half = field.shape[-1] // 2
    quarter = half // 2
    first = field[..., :half]
    second = field[..., half:]
    turned = jnp.concatenate(
        [
            -first[..., quarter:],
            first[..., :quarter],
            -second[..., quarter:],
            second[..., :quarter],
        ],
        axis=-1,
    )
    return field * cosine_table[:, None, :] + turned * sine_table[:, None, :]


def per_head_norm(field, gain):
    floats = field.astype(jnp.float32)
    return floats * lax.rsqrt(jnp.mean(floats * floats, axis=-1, keepdims=True) + norm_eps) * gain


def local(
    queries,
    keys,
    values,
    query_gain,
    key_norm_gain,
    out_weight,
    residual,
    mixer_gain,
    gate_weight,
    up_weight,
    conv_taps,
    down_weight,
):
    tok_rows = queries.shape[0]
    head_dim = query_gain.shape[0]
    heads_here = queries.shape[1] // head_dim
    kv_here = keys.shape[1] // head_dim
    query_group = heads_here // kv_here
    part_rows = tok_rows // lax.axis_size("tp")
    positions = lax.axis_index("sp") * tok_rows + jnp.arange(tok_rows, dtype=jnp.int32)
    cosine_table, sine_table = angle_tables(positions, head_dim)
    rotated_queries = apply_rotary(
        per_head_norm(queries.reshape(tok_rows, heads_here, head_dim), query_gain),
        cosine_table,
        sine_table,
    ).astype(jnp.bfloat16)
    rotated_keys = apply_rotary(
        per_head_norm(keys.reshape(tok_rows, kv_here, head_dim), key_norm_gain),
        cosine_table,
        sine_table,
    ).astype(jnp.bfloat16)
    key_flat = rotated_keys.reshape(tok_rows, kv_here * head_dim)
    query_mat = jnp.transpose(
        rotated_queries.reshape(tok_rows, kv_here, query_group, head_dim), (1, 2, 0, 3)
    )
    query_mat = query_mat.reshape(kv_here, query_group * tok_rows, head_dim)
    scale = head_dim ** (-0.5)
    start_state = (
        jnp.full((kv_here, query_group * tok_rows), -jnp.inf, jnp.float32),
        jnp.zeros((kv_here, query_group * tok_rows), jnp.float32),
        jnp.zeros((kv_here, query_group * tok_rows, head_dim), jnp.float32),
    )
    key_piece = lax.all_gather(key_flat, "sp", axis=0, tiled=True)
    value_piece = lax.all_gather(values, "sp", axis=0, tiled=True)
    piece_rows = key_piece.shape[0]
    block_slice = math.gcd(piece_rows, 512)
    key_blocks = key_piece.reshape(piece_rows // block_slice, block_slice, kv_here, head_dim)
    value_blocks = value_piece.reshape(piece_rows // block_slice, block_slice, kv_here, head_dim)

    def one_block(state, block_pair):
        running, totals, accum = state
        key_block, value_block = block_pair
        scores = (
            jnp.einsum("hqd,khd->hqk", query_mat, key_block, preferred_element_type=jnp.float32)
            * scale
        )
        new_max = jnp.maximum(running, jnp.max(scores, axis=-1))
        factor = jnp.exp(running - new_max)
        expo = jnp.exp(scores - new_max[..., None])
        totals = totals * factor + jnp.sum(expo, axis=-1)
        accum = accum * factor[..., None] + jnp.einsum(
            "hqk,khd->hqd",
            expo.astype(jnp.bfloat16),
            value_block,
            preferred_element_type=jnp.float32,
        )
        return ((new_max, totals, accum), None)

    result, unused = lax.scan(one_block, start_state, (key_blocks, value_blocks))
    running, totals, accum = result
    heads = (accum / totals[..., None]).astype(jnp.bfloat16)
    heads = jnp.transpose(heads.reshape(kv_here, query_group, tok_rows, head_dim), (2, 0, 1, 3))
    heads = heads.reshape(tok_rows, heads_here * head_dim)
    own_start = lax.axis_index("tp") * part_rows
    full_proj = lax.psum(
        jnp.dot(heads, out_weight, preferred_element_type=jnp.float32).astype(jnp.bfloat16), "tp"
    ).astype(jnp.float32)
    mixed = residual.astype(jnp.float32) + full_proj
    normed = per_head_norm(mixed, mixer_gain).astype(jnp.bfloat16)
    mixed_keep = lax.dynamic_slice_in_dim(mixed, own_start, part_rows, 0)
    gate_acc = jnp.dot(
        normed,
        lax.all_gather(gate_weight, "sp", axis=0, tiled=True),
        preferred_element_type=jnp.float32,
    )
    up_acc = jnp.dot(
        normed,
        lax.all_gather(up_weight, "sp", axis=0, tiled=True),
        preferred_element_type=jnp.float32,
    )
    gate = gate_acc.astype(jnp.bfloat16)
    up_val = up_acc.astype(jnp.bfloat16)
    padded = padded_2(gate, (("sp", 0),), 1).astype(jnp.float32)
    conv = conv_taps[0] * padded[:-2] + conv_taps[1] * padded[1:-1] + conv_taps[2] * padded[2:]
    hidden = (jax.nn.silu(conv) * up_val.astype(jnp.float32)).astype(jnp.bfloat16)
    down_full = lax.all_gather(down_weight, "sp", axis=1, tiled=True)
    mixer_out = lax.psum_scatter(
        jnp.dot(hidden, down_full, preferred_element_type=jnp.float32).astype(jnp.bfloat16),
        "tp",
        scatter_dimension=0,
        tiled=True,
    ).astype(jnp.float32)
    return (mixed_keep + mixer_out).astype(jnp.bfloat16)


def solution(mesh):
    in_specs = (
        P(("grp", "sp"), "tp"),
        P(("grp", "sp"), "tp"),
        P(("grp", "sp"), "tp"),
        P(),
        P(),
        P("tp", None),
        P(("grp", "sp"), None),
        P(),
        P("sp", "tp"),
        P("sp", "tp"),
        P(None, "tp"),
        P("tp", "sp"),
    )
    out_specs = P(("grp", "sp", "tp"), None)
    return jax.shard_map(local, mesh=mesh, in_specs=in_specs, out_specs=out_specs, check_vma=False)
```

profile of v0, /device:TPU:0, one launch (start us, length us, event | category | flops | bytes accessed | tf_op | source)
XLA Modules:
  0.0 424.0 jit_solution(16997622798966750573)
XLA Ops:
  7.4 1.3 reshape.324
  8.7 1.9 reshape.323
  10.6 1.0 fusion.32
  11.5 0.9 fusion.34
  13.4 0.9 fusion.28
  14.5 0.6 fusion.37
  15.2 1.2 fusion.31
  16.4 15.7 %all_gather.15 = bf16[1024,128]{1,0:T(8,128)(2,1)S(1)} all-gather(bf16[256,128]{1,0:T(8,128)(2,1)S(1)} %get-tuple-element.109), channel_id=1, replica_groups=mesh['grp'=2,'sp'=4,'tp'=4] {'sp'}, dimensions={0}, use_global_device_ids=true | all-gather | bytes 327680 | tf_op jit(solution)/shard_map/all_gather | solution.py:101
  32.0 14.6 %all_gather.16 = bf16[1024,128]{1,0:T(8,128)(2,1)S(1)} all-gather(bf16[256,128]{1,0:T(8,128)(2,1)S(1)} %copy-done.4), channel_id=1, replica_groups=mesh['grp'=2,'sp'=4,'tp'=4] {'sp'}, dimensions={0}, use_global_device_ids=true | all-gather | bytes 327680 | tf_op jit(solution)/shard_map/all_gather | solution.py:102
  46.6 9.3 %while.15 = (s32[]{:T(128)}, f32[1,1024]{1,0:T(1,128)S(1)}, f32[1,1024]{1,0:T(1,128)S(1)}, f32[1,1024,128]{2,1,0:T(8,128)S(1)}, bf16[2,512,1,128]{3,1,2,0:T(8,12...) while((s32[]{:T(128)}, f32[1,1024]{1,0:T(1,128)S(1)}, ...), condition=%wide.region_5.6_spmd.clone, body=%wide.region_2.5_spmd.clone.sunk | while | flops 273028096 | bytes 16318605 | solution.py:127
  46.6 1.8 multiply_reduce_fusion.4
  48.4 2.1 fusion.63
  50.6 0.6 fusion.65
  51.3 1.8 multiply_reduce_fusion.4
  53.1 2.1 fusion.63
  55.3 0.6 fusion.65
  56.3 1.7 convolution_convert_fusion
  58.7 0.5 all-gather.6.cloned.1.call-update
  59.2 0.5 all-gather.8.cloned.1.call-update
  59.8 35.8 %all-reduce.2.cloned.1.call-done = bf16[256,2048]{1,0:T(8,128)(2,1)} async-done(((bf16[256,2048]{1,0:T(8,128)(2,1)}), bf16[256,2048]{1,0:T(8,128)(2,1)}) %all-reduce.2.cloned.1.call-update) | async-done | bytes 1048592 | tf_op jit(solution)/shard_map/psum | solution.py:133
  95.7 3.2 convert_add_fusion
  98.9 68.7 %all-gather.4.cloned.1.call-done = bf16[2048,1408]{1,0:T(8,128)(2,1)} async-done(((bf16[512,1408]{1,0:T(8,128)(2,1)}), bf16[2048,1408]{1,0:T(8,128)(2,1)}) %all-gather.4.cloned.1.call-update) | async-done | bytes 5767184 | tf_op jit(solution)/shard_map/all_gather | solution.py:141
  167.6 5.1 %convolution_convert_fusion.2 = bf16[256,1408]{1,0:T(8,128)(2,1)S(1)} fusion(bf16[2048,1408]{1,0:T(8,128)(2,1)} %all-gather.4.cloned.1.call-done, f32[2048]{0:T(1024)S(1)} %copy-done.8, f32[256]{0:T(256)S(1)} %add_rsqrt_fusion.1, bf16[256,2048]{1,0:T(8,128)(2,1)} %all-reduce.2.cloned.1.call-done, bf16[256,2048]{1,0:T(8,128)(2,1)} %param.20), kind=kOutput, calls=%fused_computation.29 | convolution fusion | flops 1479901184 | bytes 8594432 | tf_op jit(solution)/shard_map/dot_general | solution.py:139
  172.8 1.3 collective-permute-start
  174.1 1.5 collective-permute-start.1
  175.6 4.0 collective-permute-done.1
  179.6 1.3 maximum_convert_fusion
  180.9 93.1 %all-gather.6.cloned.1.call-done = bf16[2048,1408]{1,0:T(8,128)(2,1)} async-done(((bf16[512,1408]{1,0:T(8,128)(2,1)}), bf16[2048,1408]{1,0:T(8,128)(2,1)}) %all-gather.6.cloned.1.call-update) | async-done | bytes 5767184 | tf_op jit(solution)/shard_map/all_gather | solution.py:146
  274.0 106.2 %all-gather.8.cloned.1.call-done = bf16[1408,2048]{1,0:T(8,128)(2,1)} async-done(((bf16[1408,512]{1,0:T(8,128)(2,1)}), bf16[1408,2048]{1,0:T(8,128)(2,1)}) %all-gather.8.cloned.1.call-update) | async-done | bytes 5767184 | tf_op jit(solution)/shard_map/all_gather | solution.py:154
  380.2 11.1 %convolution_convert_fusion.3 = bf16[256,2048]{1,0:T(8,128)(2,1)} fusion(bf16[1408,2048]{1,0:T(8,128)(2,1)} %all-gather.8.cloned.1.call-done, bf16[2048,1408]{1,0:T(8,128)(2,1)} %all-gather.6.cloned.1.call-done, f32[258,1408]{1,0:T(8,128)} %maximum_convert_fusion, f32[1408]{0:T(1024)S(1)} %get-tuple-element.91, f32[1408]{0:T(1024)S(1)} %get-tuple-element.92, ...), kind=kOutput, calls=%fused_computation.30 | convolution fusion | flops 2961145856 | bytes 19031552 | tf_op jit(solution)/shard_map/dot_general | solution.py:156
  391.3 23.2 %reduce-scatter.2.cloned.1.call-done = bf16[64,2048]{1,0:T(8,128)(2,1)} async-done(((bf16[256,2048]{1,0:T(8,128)(2,1)}), bf16[64,2048]{1,0:T(8,128)(2,1)}) %reduce-scatter.2.cloned.1.call-update) | async-done | bytes 262160 | tf_op jit(solution)/shard_map/reduce_scatter | solution.py:155
  414.5 1.9 add_convert_fusion
  (52 shorter events, 2.5 us)
Async XLA Ops:
  7.4 48.9 %copy-start = (bf16[512,2048]{1,0:T(8,128)(2,1)S(1)}, bf16[512,2048]{1,0:T(8,128)(2,1)}, u32[]{:S(2)}) copy-start(bf16[512,2048]{1,0:T(8,128)(2,1)} %param.19) | copy-start | bytes 6291460
  7.4 5.7 %copy-start.7 = (f32[128]{0:T(128)S(1)}, f32[128]{0:T(128)}, u32[]{:S(2)}) copy-start(f32[128]{0:T(128)} %param.17) | copy-start | bytes 1540
  7.4 88.3 %all-reduce.2.cloned.1.call-start = ((), (), s32[]{:S(2)}) async-start(), calls=%async_computation.1 | async-start | bytes 2097152 | tf_op jit(solution)/shard_map/psum | solution.py:133
  13.4 1.1 copy-start.3
  13.4 1.1 copy-start.6
  13.4 1.7 copy-start.2
  15.1 16.9 %copy-start.4 = (bf16[256,128]{1,0:T(8,128)(2,1)S(1)}, bf16[256,128]{1,0:T(8,128)(2,1)}, u32[]{:S(2)}) copy-start(bf16[256,128]{1,0:T(8,128)(2,1)} %param.16) | copy-start | bytes 196612
  48.4 2.2 copy-start.1
  53.0 2.2 copy-start.1
  58.0 109.6 %all-gather.4.cloned.1.call-start = ((), (), s32[]{:S(2)}) async-start(), calls=%async_computation.2 | async-start | bytes 7208960 | tf_op jit(solution)/shard_map/all_gather | solution.py:141
  58.6 215.4 %all-gather.6.cloned.1.call-start = ((), (), s32[]{:S(2)}) async-start(), calls=%async_computation.3 | async-start | bytes 7208960 | tf_op jit(solution)/shard_map/all_gather | solution.py:146
  59.2 321.0 %all-gather.8.cloned.1.call-start = ((), (), s32[]{:S(2)}) async-start(), calls=%async_computation.4 | async-start | bytes 7208960 | tf_op jit(solution)/shard_map/all_gather | solution.py:154
  59.8 107.8 %copy-start.8 = (f32[2048]{0:T(1024)S(1)}, f32[2048]{0:T(1024)}, u32[]{:S(2)}) copy-start(f32[2048]{0:T(1024)} %param.21) | copy-start | bytes 24580
  59.8 354.7 %reduce-scatter.2.cloned.1.call-start = ((), (), s32[]{:S(2)}) async-start(), calls=%async_computation.5 | async-start | bytes 1310720 | tf_op jit(solution)/shard_map/reduce_scatter | solution.py:155
  98.9 76.6 %copy-start.5 = (f32[3,1408]{1,0:T(4,128)S(1)}, f32[3,1408]{1,0:T(4,128)}, u32[]{:S(2)}) copy-start(f32[3,1408]{1,0:T(4,128)} %param.24) | copy-start | bytes 50692
  172.8 2.8 collective-permute-start
  174.1 5.5 %collective-permute-start.1 = (bf16[1,1408]{1,0:T(2,128)(2,1)S(1)}, bf16[1,1408]{1,0:T(2,128)(2,1)S(1)}, u32[]{:S(2)}, u32[]{:S(2)}) collective-permute-start(bf16[1,1408]{1,0:T(2,128)(2,1)S(1)} %get-tuple-element.117), channel_id=1, source_target_pairs={{4,0},{8,4},{12,8},{5,1},{9,5},{13,9},{6,2},{10,6},{14,10},{7,3},{... | collective-permute-start | bytes 8456 | tf_op jit(solution)/shard_map/ppermute | solution.py:20
Sparse Core Ops, SparseCore 0:
  58.1 37.4 all-reduce.1
  391.4 23.0 reduce-scatter.1
Sparse Core Ops, SparseCore 1:
  60.1 107.5 all-gather.3
  169.0 104.9 all-gather.5
  275.4 104.7 all-gather.7
where the time goes:
time: 424 us
  waiting for transfers between devices  333 us (79%)
  blocking collectives  30.2 us (7%)
  matrix products  22.8 us (5%)
  other arithmetic  16.5 us (4%)
  between operations  15.3 us (4%)
    all_gather x1, waiting for transfers between devices, local(): down_full = lax.all_gather(down_weight, 'sp', axis=1, tiled=True)  106 us
    all_gather x1, waiting for transfers between devices, local(): lax.all_gather(up_weight, 'sp', axis=0, tiled=True)  93.1 us
    all_gather x1, waiting for transfers between devices, local(): lax.all_gather(gate_weight, 'sp', axis=0, tiled=True)  68.7 us
    psum x1, waiting for transfers between devices, local(): lax.psum(jnp.dot(heads, out_weight, preferred_element_type=jnp.float32).a...  35.8 us
    reduce_scatter x1, waiting for transfers between devices, local(): lax.psum_scatter(jnp.dot(hidden, down_full, preferred_element_type=jnp.fl...  23.2 us
    all_gather x1, blocking collectives, local(): key_piece = lax.all_gather(key_flat, 'sp', axis=0, tiled=True)  15.7 us
    all_gather x1, blocking collectives, local(): value_piece = lax.all_gather(values, 'sp', axis=0, tiled=True)  14.6 us
    dot_general x1, matrix products, local(): jnp.dot(hidden, down_full, preferred_element_type=jnp.float32)  11.1 us
  transfers between devices with their start and end apart: 7, of which 6 were waited for; matrix products, arithmetic and copies ran while one was open for 2% of the time, Pallas kernels for 0%

commit v1 on v0

--- a/solution.py
+++ b/solution.py
@@ -1,3 +1,4 @@
+import functools
 import math
 import jax
 import jax.numpy as jnp
@@ -7,6 +8,22 @@
 GRID = 64
 norm_eps = 1e-06
 rope_base = 10000.0
+
+
+def _raise_sides(u, axis_no):
+    n_chips = lax.psum(1, axis_name="sp")
+    inter = sorted(((ix, (ix + 1) % n_chips) for ix in range(n_chips)))
+    piece_now = u
+    rack = [piece_now]
+    for ii in [*range(1, n_chips)]:
+        piece_now = lax.ppermute(piece_now, axis_name="sp", perm=inter)
+        rack.insert(0, piece_now)
+    val = jnp.concatenate(rack, axis=axis_no)
+    upper = jnp.roll(val, (lax.axis_index("sp") + 1) * u.shape[axis_no], axis=axis_no)
+    return upper
+
+
+masks_bind = functools.partial(_raise_sides, axis_no=1)
 
 
 def padded_2(block, sides, width):
@@ -151,7 +168,7 @@
     padded = padded_2(gate, (("sp", 0),), 1).astype(jnp.float32)
     conv = conv_taps[0] * padded[:-2] + conv_taps[1] * padded[1:-1] + conv_taps[2] * padded[2:]
     hidden = (jax.nn.silu(conv) * up_val.astype(jnp.float32)).astype(jnp.bfloat16)
-    down_full = lax.all_gather(down_weight, "sp", axis=1, tiled=True)
+    down_full = masks_bind(down_weight)
     mixer_out = lax.psum_scatter(
         jnp.dot(hidden, down_full, preferred_element_type=jnp.float32).astype(jnp.bfloat16),
         "tp",

time: 424 us -> 384 us (0.906)
  waiting for transfers between devices: 333 us -> 242 us
  starting transfers between devices: 2.93 us -> 32.3 us
  local copies, waits for them, and re-layouts: 3.61 us -> 22.2 us
    ppermute x0 -> x3, waiting for transfers between devices: none -> 159 us  [_raise_sides(): piece_now = lax.ppermute(piece_now, axis_name='sp', perm=inter)]
    all_gather x1 -> x0, waiting for transfers between devices: 106 us -> none  [local(): down_full = lax.all_gather(down_weight, 'sp', axis=1, tiled=True)]
    all_gather x1, waiting for transfers between devices: 68.7 us -> 0.01 us  [local(): lax.all_gather(gate_weight, 'sp', axis=0, tiled=True)]
    psum x1, waiting for transfers between devices: 35.8 us -> 0.01 us  [local(): lax.psum(jnp.dot(heads, out_weight, preferred_element_type=jnp.float32).a...]
    all_gather x1, waiting for transfers between devices: 93.1 us -> 58.1 us  [local(): lax.all_gather(up_weight, 'sp', axis=0, tiled=True)]
    ppermute x0 -> x3, starting transfers between devices: none -> 26.2 us  [_raise_sides(): piece_now = lax.ppermute(piece_now, axis_name='sp', perm=inter)]
    unnamed x16 -> x25, local copies, waits for them, and re-layouts: 0.04 us -> 16 us
  transfers between devices with their start and end apart: 7 -> 9, of which waited for: 6 -> 5; matrix products, arithmetic and copies ran while one was open for 2% -> 7% of each run, Pallas kernels for 0% -> 0%
where the time goes in v1:
time: 384 us; the launch traced here: 383 us
  waiting for transfers between devices  242 us (63%)
  starting transfers between devices  32.3 us (8%)
  blocking collectives  30.1 us (8%)
  matrix products  23.1 us (6%)
  local copies, waits for them, and re-layouts  22.2 us (6%)
  other arithmetic  18.9 us (5%)
  between operations  15.1 us (4%)
    ppermute x3, waiting for transfers between devices, _raise_sides(): piece_now = lax.ppermute(piece_now, axis_name='sp', perm=inter)  159 us
    all_gather x1, waiting for transfers between devices, local(): lax.all_gather(up_weight, 'sp', axis=0, tiled=True)  58.1 us
    ppermute x3, starting transfers between devices, _raise_sides(): piece_now = lax.ppermute(piece_now, axis_name='sp', perm=inter)  26.2 us
    reduce_scatter x1, waiting for transfers between devices, local(): lax.psum_scatter(jnp.dot(hidden, down_full, preferred_element_type=jnp.fl...  23.5 us
    unnamed x25, local copies, waits for them, and re-layouts  16 us
    all_gather x1, blocking collectives, local(): key_piece = lax.all_gather(key_flat, 'sp', axis=0, tiled=True)  15.7 us
    all_gather x1, blocking collectives, local(): value_piece = lax.all_gather(values, 'sp', axis=0, tiled=True)  14.4 us
    dot_general x1, matrix products, local(): jnp.dot(hidden, down_full, preferred_element_type=jnp.float32)  11.4 us
  transfers between devices with their start and end apart: 9, of which 5 were waited for; matrix products, arithmetic and copies ran while one was open for 7% of the time, Pallas kernels for 0%

profile of v1, /device:TPU:0, one launch (start us, length us, event | category | flops | bytes accessed | tf_op | source)
XLA Modules:
  0.0 383.4 jit_solution(6215482838377324401)
XLA Ops:
  8.7 1.9 reshape.323
  13.6 1.7 fusion.42
  15.4 15.7 %all_gather.12 = bf16[1024,128]{1,0:T(8,128)(2,1)S(1)} all-gather(bf16[256,128]{1,0:T(8,128)(2,1)S(1)} %get-tuple-element.109), channel_id=1, replica_groups=mesh['grp'=2,'sp'=4,'tp'=4] {'sp'}, dimensions={0}, use_global_device_ids=true | all-gather | bytes 327680 | tf_op jit(solution)/shard_map/all_gather | solution.py:118
  34.0 14.4 %all_gather.13 = bf16[1024,128]{1,0:T(8,128)(2,1)S(1)} all-gather(bf16[256,128]{1,0:T(8,128)(2,1)S(1)} %copy-done.7), channel_id=1, replica_groups=mesh['grp'=2,'sp'=4,'tp'=4] {'sp'}, dimensions={0}, use_global_device_ids=true | all-gather | bytes 327680 | tf_op jit(solution)/shard_map/all_gather | solution.py:119
  48.4 9.3 %while.15 = (s32[]{:T(128)}, f32[1,1024]{1,0:T(1,128)S(1)}, f32[1,1024]{1,0:T(1,128)S(1)}, f32[1,1024,128]{2,1,0:T(8,128)S(1)}, bf16[2,512,1,128]{3,1,2,0:T(8,12...) while((s32[]{:T(128)}, f32[1,1024]{1,0:T(1,128)S(1)}, ...), condition=%wide.region_5.6_spmd.clone, body=%wide.region_2.5_spmd.clone.sunk | while | flops 273028096 | bytes 16318613 | solution.py:144
  48.4 1.8 multiply_reduce_fusion.4
  50.2 2.1 fusion.68
  53.1 1.8 multiply_reduce_fusion.4
  54.9 2.1 fusion.68
  58.1 1.7 convolution_convert_fusion
  61.2 1.5 collective-permute-start.2
  62.7 51.8 %collective-permute-done.2 = bf16[1408,512]{1,0:T(8,128)(2,1)S(1)} collective-permute-done((bf16[1408,512]{1,0:T(8,128)(2,1)S(1)}, bf16[1408,512]{1,0:T(8,128)(2,1)S(1)}, u32[]{:S(2)}, u32[]{:S(2)}) %collective-permute-start.2) | collective-permute-done | bytes 1441824 | tf_op jit(solution)/shard_map/ppermute | solution.py:19
  115.6 14.2 %collective-permute-start.3 = (bf16[1408,512]{1,0:T(8,128)(2,1)S(1)}, bf16[1408,512]{1,0:T(8,128)(2,1)}, u32[]{:S(2)}, u32[]{:S(2)}) collective-permute-start(bf16[1408,512]{1,0:T(8,128)(2,1)S(1)} %collective-permute-done.2), channel_id=1, source_target_pairs={{0,4},{4,8},{8,12},{12,0},{1,5},{5,9},{9,13},{13,1},{2,6},{6,10},{... | collective-permute-start | bytes 4325384 | tf_op jit(solution)/shard_map/ppermute | solution.py:19
  129.8 69.7 %collective-permute-done.3 = bf16[1408,512]{1,0:T(8,128)(2,1)} collective-permute-done((bf16[1408,512]{1,0:T(8,128)(2,1)S(1)}, bf16[1408,512]{1,0:T(8,128)(2,1)}, u32[]{:S(2)}, u32[]{:S(2)}) %collective-permute-start.3) | collective-permute-done | bytes 1441824 | tf_op jit(solution)/shard_map/ppermute | solution.py:19
  199.5 10.4 %collective-permute-start.4 = (bf16[1408,512]{1,0:T(8,128)(2,1)}, bf16[1408,512]{1,0:T(8,128)(2,1)}, u32[]{:S(2)}, u32[]{:S(2)}) collective-permute-start(bf16[1408,512]{1,0:T(8,128)(2,1)} %collective-permute-done.3), channel_id=1, source_target_pairs={{0,4},{4,8},{8,12},{12,0},{1,5},{5,9},{9,13},{13,1},{2,6},{6,10},{... | collective-permute-start | bytes 4325384 | tf_op jit(solution)/shard_map/ppermute | solution.py:19
  210.0 1.5 slice_reduce_fusion.2
  211.5 3.2 convert_add_fusion
  215.2 37.5 %collective-permute-done.4 = bf16[1408,512]{1,0:T(8,128)(2,1)} collective-permute-done((bf16[1408,512]{1,0:T(8,128)(2,1)}, bf16[1408,512]{1,0:T(8,128)(2,1)}, u32[]{:S(2)}, u32[]{:S(2)}) %collective-permute-start.4) | collective-permute-done | bytes 1441824 | tf_op jit(solution)/shard_map/ppermute | solution.py:19
  252.7 2.6 constant_dynamic-update-slice_fusion.7
  255.3 2.8 constant_dynamic-update-slice_fusion.6
  258.1 1.3 constant_dynamic-update-slice_fusion.5
  260.7 2.7 constant_dynamic-update-slice_fusion.3
  263.3 2.7 constant_dynamic-update-slice_fusion.2
  266.0 1.3 constant_dynamic-update-slice_fusion.1
  267.3 5.2 %convolution_convert_fusion.2 = bf16[256,1408]{1,0:T(8,128)(2,1)S(1)} fusion(bf16[2048,1408]{1,0:T(8,128)(2,1)} %all-gather.3.cloned.1.call-done, f32[2048]{0:T(1024)} %param.21, f32[256]{0:T(256)} %add_rsqrt_fusion.1, bf16[256,2048]{1,0:T(8,128)(2,1)} %all-reduce.2.cloned.1.call-done, bf16[256,2048]{1,0:T(8,128)(2,1)} %param.20), kind=kOutput, calls=%fused_computation.32 | convolution fusion | flops 1479901184 | bytes 8594432 | tf_op jit(solution)/shard_map/dot_general | solution.py:156
  272.5 1.3 collective-permute-start.1
  273.8 4.7 %collective-permute-start = (bf16[1,1408]{1,0:T(2,128)(2,1)S(1)}, bf16[1,1408]{1,0:T(2,128)(2,1)S(1)}, u32[]{:S(2)}, u32[]{:S(2)}) collective-permute-start(bf16[1,1408]{1,0:T(2,128)(2,1)S(1)} %get-tuple-element.116), channel_id=1, source_target_pairs={{0,4},{4,8},{8,12},{1,5},{5,9},{9,13},{2,6},{6,10},{10,14},{3,7},{... | collective-permute-start | bytes 8456 | tf_op jit(solution)/shard_map/ppermute | solution.py:34
  279.8 1.3 maximum_convert_fusion
  281.1 58.1 %all-gather.5.cloned.1.call-done = bf16[2048,1408]{1,0:T(8,128)(2,1)} async-done(((bf16[512,1408]{1,0:T(8,128)(2,1)}), bf16[2048,1408]{1,0:T(8,128)(2,1)}) %all-gather.5.cloned.1.call-update) | async-done | bytes 5767184 | tf_op jit(solution)/shard_map/all_gather | solution.py:163
  339.2 11.4 %fusion.20 = bf16[256,2048]{1,0:T(8,128)(2,1)} fusion(bf16[1408,4096]{1,0:T(8,128)(2,1)} %constant_dynamic-update-slice_fusion, s32[]{:T(128)S(6)} %select_n.39, bf16[2048,1408]{1,0:T(8,128)(2,1)} %all-gather.5.cloned.1.call-done, f32[258,1408]{1,0:T(8,128)} %maximum_convert_fusion, f32[1408]{0:T(1024)S(1)} %get-tuple-element.91, ...), kind=kOutput, calls=%fused_computation.27 | convolution fusion | flops 2961145856 | bytes 19034116 | tf_op jit(solution)/shard_map/dot_general | solution.py:173
  350.6 23.5 %reduce-scatter.2.cloned.1.call-done = bf16[64,2048]{1,0:T(8,128)(2,1)} async-done(((bf16[256,2048]{1,0:T(8,128)(2,1)}), bf16[64,2048]{1,0:T(8,128)(2,1)}) %reduce-scatter.2.cloned.1.call-update) | async-done | bytes 262160 | tf_op jit(solution)/shard_map/reduce_scatter | solution.py:172
  374.1 1.9 add_convert_fusion
  (65 shorter events, 14.5 us)
Async XLA Ops:
  7.4 50.7 %copy-start = (bf16[512,2048]{1,0:T(8,128)(2,1)S(1)}, bf16[512,2048]{1,0:T(8,128)(2,1)}, u32[]{:S(2)}) copy-start(bf16[512,2048]{1,0:T(8,128)(2,1)} %param.19) | copy-start | bytes 6291460
  7.4 6.2 %copy-start.6 = (bf16[256,128]{1,0:T(8,128)(2,1)S(1)}, bf16[256,128]{1,0:T(8,128)(2,1)}, u32[]{:S(2)}) copy-start(bf16[256,128]{1,0:T(8,128)(2,1)} %param.15) | copy-start | bytes 196612
  7.4 6.2 %copy-start.8 = (f32[128]{0:T(128)S(1)}, f32[128]{0:T(128)}, u32[]{:S(2)}) copy-start(f32[128]{0:T(128)} %param.18) | copy-start | bytes 1540
  7.4 204.1 %all-reduce.2.cloned.1.call-start = ((), (), s32[]{:S(2)}) async-start(), calls=%async_computation.1 | async-start | bytes 2097152 | tf_op jit(solution)/shard_map/psum | solution.py:150
  10.6 20.8 %copy-start.9 = (f32[128]{0:T(128)S(1)}, f32[128]{0:T(128)}, u32[]{:S(2)}) copy-start(f32[128]{0:T(128)} %param.17) | copy-start | bytes 1540
  31.8 1.0 copy-start.5
  32.6 1.4 copy-start.7
  50.2 2.2 copy-start.1
  54.9 2.2 copy-start.1
  59.8 1.4 copy-start.2
  59.9 207.4 %all-gather.3.cloned.1.call-start = ((), (), s32[]{:S(2)}) async-start(), calls=%async_computation.2 | async-start | bytes 7208960 | tf_op jit(solution)/shard_map/all_gather | solution.py:158
  60.5 278.8 %all-gather.5.cloned.1.call-start = ((), (), s32[]{:S(2)}) async-start(), calls=%async_computation.3 | async-start | bytes 7208960 | tf_op jit(solution)/shard_map/all_gather | solution.py:163
  61.0 313.1 %reduce-scatter.2.cloned.1.call-start = ((), (), s32[]{:S(2)}) async-start(), calls=%async_computation.4 | async-start | bytes 1310720 | tf_op jit(solution)/shard_map/reduce_scatter | solution.py:172
  61.2 53.3 %collective-permute-start.2 = (bf16[1408,512]{1,0:T(8,128)(2,1)S(1)}, bf16[1408,512]{1,0:T(8,128)(2,1)S(1)}, u32[]{:S(2)}, u32[]{:S(2)}) collective-permute-start(bf16[1408,512]{1,0:T(8,128)(2,1)S(1)} %copy-done.2), channel_id=1, source_target_pairs={{0,4},{4,8},{8,12},{12,0},{1,5},{5,9},{9,13},{13,1},{2,6},{6,10},{... | collective-permute-start | bytes 4325384 | tf_op jit(solution)/shard_map/ppermute | solution.py:19
  114.5 1.1 copy-start.3
  115.6 83.9 %collective-permute-start.3 = (bf16[1408,512]{1,0:T(8,128)(2,1)S(1)}, bf16[1408,512]{1,0:T(8,128)(2,1)}, u32[]{:S(2)}, u32[]{:S(2)}) collective-permute-start(bf16[1408,512]{1,0:T(8,128)(2,1)S(1)} %collective-permute-done.2), channel_id=1, source_target_pairs={{0,4},{4,8},{8,12},{12,0},{1,5},{5,9},{9,13},{13,1},{2,6},{6,10},{... | collective-permute-start | bytes 4325384 | tf_op jit(solution)/shard_map/ppermute | solution.py:19
  199.5 53.2 %collective-permute-start.4 = (bf16[1408,512]{1,0:T(8,128)(2,1)}, bf16[1408,512]{1,0:T(8,128)(2,1)}, u32[]{:S(2)}, u32[]{:S(2)}) collective-permute-start(bf16[1408,512]{1,0:T(8,128)(2,1)} %collective-permute-done.3), channel_id=1, source_target_pairs={{0,4},{4,8},{8,12},{12,0},{1,5},{5,9},{9,13},{13,1},{2,6},{6,10},{... | collective-permute-start | bytes 4325384 | tf_op jit(solution)/shard_map/ppermute | solution.py:19
  255.3 2.8 copy-start.4
  272.5 7.3 %collective-permute-start.1 = (bf16[1,1408]{1,0:T(2,128)(2,1)S(1)}, bf16[1,1408]{1,0:T(2,128)(2,1)S(1)}, u32[]{:S(2)}, u32[]{:S(2)}) collective-permute-start(bf16[1,1408]{1,0:T(2,128)(2,1)S(1)} %get-tuple-element.117), channel_id=1, source_target_pairs={{4,0},{8,4},{12,8},{5,1},{9,5},{13,9},{6,2},{10,6},{14,10},{7,3},{... | collective-permute-start | bytes 8456 | tf_op jit(solution)/shard_map/ppermute | solution.py:37
  273.8 6.0 %collective-permute-start = (bf16[1,1408]{1,0:T(2,128)(2,1)S(1)}, bf16[1,1408]{1,0:T(2,128)(2,1)S(1)}, u32[]{:S(2)}, u32[]{:S(2)}) collective-permute-start(bf16[1,1408]{1,0:T(2,128)(2,1)S(1)} %get-tuple-element.116), channel_id=1, source_target_pairs={{0,4},{4,8},{8,12},{1,5},{5,9},{9,13},{2,6},{6,10},{10,14},{3,7},{... | collective-permute-start | bytes 8456 | tf_op jit(solution)/shard_map/ppermute | solution.py:34
Sparse Core Ops, SparseCore 0:
  60.0 37.5 all-reduce.1
  350.7 23.3 reduce-scatter.1
Sparse Core Ops, SparseCore 1:
  61.9 165.3 all-gather.2
  228.7 110.5 all-gather.4
